TPU v7x, 32 devices: a whole 2x2x4 slice. The times are simulated.
32 devices in a mesh: row: 8 (over z, y), col: 4 (over x, core).
Axes of the slice: x: 2, y: 2, z: 4, core: 2. Of those that a mesh axis runs over, the one named last changes fastest.
Arguments:
- tokens: bfloat16 [16384, 2048], P(('row', 'col')), may hold values from -6 to 6
- w_mix: bfloat16 [2048, 512], replicated, may hold values from -0.125 to 0.125
- w_gate: bfloat16 [2048, 2048], replicated, may hold values from -0.125 to 0.125
- gate_bias: float32 [2048], replicated, may hold values from -4 to 4
- w_branch: bfloat16 [512, 2048], replicated, may hold values from -0.25 to 0.25
Outputs:
- mixed: bfloat16 [16384, 2048], P(('row', 'col'))
All inputs are finite; a program needn't handle non-finite values.
Results may differ from a plain program's by a relative error of at most 0.0083.
Values may be sent and summed in bfloat16 or wider, within the bound.
No kernel may reach another device: no remote copies, remote signals or barrier semaphores. Data moves between devices by JAX's collectives and lax.ppermute only.
A program may use at most 64 MiB of HBM per device.

v0:
```python
import math
import jax
import jax.numpy as jnp
from jax import lax
from jax.sharding import PartitionSpec as P

GROUP_DIM = 64
HIGH = lax.Precision.HIGHEST


def phase_table(left, right, period):
    product = left[:, None] * right[None, :] % period
    angle = product.astype(jnp.float32) * (2.0 * math.pi / period)
    return (jnp.cos(angle), jnp.sin(angle))


def group_tables(span):
    index = jnp.arange(span, dtype=jnp.int32)
    inner = index % GROUP_DIM
    cos_c, sin_c = phase_table(inner, inner, GROUP_DIM)
    same = (index[:, None] // GROUP_DIM == index[None, :] // GROUP_DIM).astype(jnp.float32)
    return (cos_c * same, sin_c * same)


def shards(tokens, w_mix, w_gate, gate_bias, w_branch):
    n_dev = lax.axis_size(("row", "col"))
    local_len = tokens.shape[0]
    full_len = local_len * n_dev
    sub_len = local_len // n_dev
    mixed_in = jnp.dot(tokens, w_mix, preferred_element_type=jnp.float32).astype(jnp.bfloat16)
    channels = mixed_in.shape[1]
    span = min(channels, max(GROUP_DIM, 128))
    pieces = lax.all_to_all(
        mixed_in.reshape(1, local_len, channels),
        ("row", "col"),
        split_axis=1,
        concat_axis=0,
        tiled=True,
    )
    values = pieces.astype(jnp.float32)
    dev_iota = jnp.arange(n_dev, dtype=jnp.int32)
    cos_p, sin_p = phase_table(dev_iota, dev_iota, n_dev)
    first_re = jnp.einsum("kn,nmc->kmc", cos_p, values, precision=HIGH)
    first_im = -jnp.einsum("kn,nmc->kmc", sin_p, values, precision=HIGH)
    cos_c, sin_c = group_tables(span)
    shaped = (n_dev, sub_len, channels // span, span)
    part_re = first_re.reshape(shaped)
    part_im = first_im.reshape(shaped)
    chan_re = jnp.einsum("kmgc,cd->kmgd", part_re, cos_c, precision=HIGH) + jnp.einsum(
        "kmgc,cd->kmgd", part_im, sin_c, precision=HIGH
    )
    chan_im = jnp.einsum("kmgc,cd->kmgd", part_im, cos_c, precision=HIGH) - jnp.einsum(
        "kmgc,cd->kmgd", part_re, sin_c, precision=HIGH
    )
    chan_re = chan_re.reshape(n_dev, sub_len, channels)
    chan_im = chan_im.reshape(n_dev, sub_len, channels)
    start = lax.axis_index(("row", "col")) * sub_len
    positions = start + jnp.arange(sub_len, dtype=jnp.int32)
    cos_t, sin_t = phase_table(dev_iota, positions, full_len)
    twist_re = chan_re * cos_t[:, :, None] + chan_im * sin_t[:, :, None]
    twist_im = chan_im * cos_t[:, :, None] - chan_re * sin_t[:, :, None]
    recv_re, recv_im = (
        lax.all_to_all(twist_re, ("row", "col"), split_axis=0, concat_axis=1, tiled=True),
        lax.all_to_all(twist_im, ("row", "col"), split_axis=0, concat_axis=1, tiled=True),
    )
    recv_re = recv_re.reshape(local_len, channels)
    recv_im = recv_im.reshape(local_len, channels)
    len_iota = jnp.arange(local_len, dtype=jnp.int32)
    cos_m, sin_m = phase_table(len_iota, len_iota, local_len)
    real_part = jnp.dot(cos_m, recv_re, precision=HIGH) + jnp.dot(sin_m, recv_im, precision=HIGH)
    real_part = real_part * (1.0 / math.sqrt(full_len * GROUP_DIM))
    freq_rows = real_part.astype(jnp.bfloat16).reshape(local_len, 1, channels)
    spectrum = lax.all_to_all(
        freq_rows, ("row", "col"), split_axis=0, concat_axis=1, tiled=True
    ).reshape(local_len, channels)
    gate = jax.nn.sigmoid(jnp.dot(tokens, w_gate, preferred_element_type=jnp.float32) + gate_bias)
    branch = jnp.dot(spectrum, w_branch, preferred_element_type=jnp.float32)
    return (gate * branch).astype(jnp.bfloat16)


def solution(mesh):
    in_specs = (P(("row", "col"), None), P(), P(), P(), P())
    out_specs = P(("row", "col"), None)
    return jax.shard_map(shards, mesh=mesh, in_specs=in_specs, out_specs=out_specs, check_vma=False)
```

profile of v0, /device:TPU:0, one launch (start us, length us, event | category | flops | bytes accessed | tf_op | source)
XLA Modules:
  0.0 156.2 jit_solution(4183638831278517337)
XLA Ops:
  0.0 0.0 copy-start
  0.0 1.6 %copy-done = bf16[512,2048]{1,0:T(8,128)(2,1)S(1)} copy-done((bf16[512,2048]{1,0:T(8,128)(2,1)S(1)}, bf16[512,2048]{1,0:T(8,128)(2,1)}, u32[]{:S(2)}) %copy-start) | copy-done | bytes 2097176
  1.6 2.8 %fusion.5 = bf16[1,512,512]{2,1,0:T(8,128)(2,1)S(1)} fusion(bf16[512,2048]{1,0:T(8,128)(2,1)S(1)} %copy-done, bf16[2048,512]{1,0:T(8,128)(2,1)} %param.6), kind=kOutput, calls=%fused_computation.14 | convolution fusion | flops 1074003968 | bytes 4718592 | tf_op jit(solution)/shard_map/dot_general | solution.py:30
  4.4 0.8 copy.68
  5.2 0.6 broadcast.262
  5.8 4.6 %reduce = bf16[512,512]{1,0:T(8,128)(2,1)} reduce(bf16[512,1,512]{2,1,0:T(2,128)(2,1)S(1)} %bitcast.70, bf16[]{:T(256)} %broadcast.262), dimensions={1}, to_apply=%bitcast.66.reduce_sub_computation | reduce | bytes 1048578
  10.4 2.2 %reshape.199 = bf16[32,2,4096]{2,1,0:T(2,128)(2,1)} reshape(bf16[512,512]{1,0:T(8,128)(2,1)} %reduce) | data formatting | bytes 1048576
  12.7 7.5 %all-to-all-start = ((bf16[32,2,4096]{2,1,0:T(2,128)(2,1)}), bf16[32,2,4096]{2,1,0:T(2,128)(2,1)S(1)}, u32[]{:S(2)}, u32[]{:S(2)}) async-start(bf16[32,2,4096]{2,1,0:T(2,128)(2,1)} %reshape.199), calls=%async_computation | async-start | bytes 1048576 | tf_op jit(solution)/shard_map/all_to_all | solution.py:33
  20.2 0.1 fusion.70
  20.3 15.3 %all-to-all-done = bf16[32,2,4096]{2,1,0:T(2,128)(2,1)S(1)} async-done(((bf16[32,2,4096]{2,1,0:T(2,128)(2,1)}), bf16[32,2,4096]{2,1,0:T(2,128)(2,1)S(1)}, u32[]{:S(2)}, u32[]{:S(2)}) %all-to-all-start) | async-done | bytes 524320 | tf_op jit(solution)/shard_map/all_to_all | solution.py:33
  35.6 1.8 %reshape.200 = bf16[512,1,512]{2,1,0:T(2,128)(2,1)} reshape(bf16[32,2,4096]{2,1,0:T(2,128)(2,1)S(1)} %all-to-all-done) | data formatting | bytes 1048576
  37.4 1.3 copy.47
  38.7 0.0 copy-start.2
  38.8 0.8 copy-done.2
  39.5 0.9 reshape.198
  40.5 1.8 %fusion.23 = f32[32,16,4,128]{3,0,2,1:T(8,128)S(1)} fusion(bf16[16,4,128,32]{2,1,0,3:T(4,128)(2,1)} %reshape.198), kind=kOutput, calls=%fused_computation.36 | convolution fusion | flops 100677632 | bytes 1572864 | tf_op jit(solution)/shard_map/kn,nmc->kmc/dot_general | solution.py:43
  42.3 2.9 %convolution_negate_fusion = f32[32,16,512]{2,0,1:T(8,128)} fusion(bf16[32,16,512]{2,1,0:T(8,128)(2,1)} %bitcast.68), kind=kOutput, calls=%fused_computation.4 | convolution fusion | flops 100939776 | bytes 1572864 | tf_op jit(solution)/shard_map/kn,nmc->kmc/dot_general | solution.py:44
  45.1 2.5 %reshape.187 = f32[32,16,4,128]{3,2,0,1:T(4,128)} reshape(f32[32,16,512]{2,0,1:T(8,128)} %convolution_negate_fusion) | data formatting | bytes 2097152 | tf_op jit(solution)/shard_map/reshape | solution.py:48
  47.7 0.0 copy-start.1
  47.7 2.0 %fusion.21 = f32[32,16,4,128]{3,1,2,0:T(8,128)S(1)} fusion(f32[32,16,4,128]{3,0,2,1:T(8,128)S(1)} %fusion.23, s32[128]{0:T(128)S(1)} %get-tuple-element.9, s32[128]{0:T(128)S(1)} %get-tuple-element.10), kind=kOutput, calls=%fused_computation.34 | convolution fusion | flops 402915328 | bytes 2098176 | tf_op jit(solution)/shard_map/kmgc,cd->kmgd/dot_general | solution.py:49
  49.6 0.0 copy-done.1
  49.7 1.8 %fusion.17 = f32[32,16,4,128]{3,1,2,0:T(8,128)S(1)} fusion(f32[32,16,4,128]{3,2,0,1:T(4,128)S(1)} %copy-done.1, s32[128]{0:T(128)S(1)} %get-tuple-element.9, s32[128]{0:T(128)S(1)} %get-tuple-element.10), kind=kOutput, calls=%fused_computation.30 | convolution fusion | flops 402915328 | bytes 2098176 | tf_op jit(solution)/shard_map/kmgc,cd->kmgd/dot_general | solution.py:52
  51.5 1.8 %fusion.2 = f32[32,4,2,8,128]{4,3,2,1,0:T(8,128)S(1)} fusion(f32[32,16,4,128]{3,1,2,0:T(8,128)S(1)} %fusion.21, f32[32,16,4,128]{3,2,0,1:T(4,128)S(1)} %copy-done.1, s32[128]{0:T(128)S(1)} %get-tuple-element.9, s32[128]{0:T(128)S(1)} %get-tuple-element.10), kind=kOutput, calls=%fused_computation.10 | convolution fusion | flops 403177472 | bytes 3146752 | tf_op jit(solution)/shard_map/kmgc,cd->kmgd/dot_general | solution.py:49
  53.3 2.0 %fusion.1 = f32[32,4,2,8,128]{4,3,2,1,0:T(8,128)S(1)} fusion(f32[32,16,4,128]{3,1,2,0:T(8,128)S(1)} %fusion.17, f32[32,16,4,128]{3,0,2,1:T(8,128)S(1)} %fusion.23, s32[128]{0:T(128)S(1)} %get-tuple-element.9, s32[128]{0:T(128)S(1)} %get-tuple-element.10), kind=kOutput, calls=%fused_computation.8 | convolution fusion | flops 403177472 | bytes 3146752 | tf_op jit(solution)/shard_map/kmgc,cd->kmgd/dot_general | solution.py:52
  55.4 1.3 fusion.10
  56.6 29.1 %all_to_all.45 = f32[32,16,512]{2,1,0:T(8,128)} all-to-all(f32[32,16,512]{2,1,0:T(8,128)S(1)} %get-tuple-element.6), channel_id=1, replica_groups=mesh['row'=8,'col'=4] {'row','col'}, dimensions={0} | all-to-all | bytes 2097152 | tf_op jit(solution)/shard_map/all_to_all | solution.py:63
  85.7 3.8 %all-to-all-start.2 = ((f32[32,16,512]{2,1,0:T(8,128)}), f32[32,16,512]{2,1,0:T(8,128)S(1)}, u32[]{:S(2)}, u32[]{:S(2)}) async-start(f32[32,16,512]{2,1,0:T(8,128)} %get-tuple-element.5), calls=%async_computation.2 | async-start | bytes 2097152 | tf_op jit(solution)/shard_map/all_to_all | solution.py:64
  89.6 8.0 %fusion.12 = f32[512,512]{1,0:T(8,128)} fusion(f32[512,512]{1,0:T(8,128)} %bitcast.73), kind=kOutput, calls=%fused_computation.25 | convolution fusion | flops 1614282752 | bytes 2097152 | tf_op jit(solution)/shard_map/dot_general | solution.py:70
  97.5 18.0 %all-to-all-done.2 = f32[32,16,512]{2,1,0:T(8,128)S(1)} async-done(((f32[32,16,512]{2,1,0:T(8,128)}), f32[32,16,512]{2,1,0:T(8,128)S(1)}, u32[]{:S(2)}, u32[]{:S(2)}) %all-to-all-start.2) | async-done | bytes 1048608 | tf_op jit(solution)/shard_map/all_to_all | solution.py:64
  115.6 7.8 %fusion.4 = bf16[512,1,512]{2,0,1:T(8,128)(2,1)} fusion(f32[512,512]{1,0:T(8,128)} %fusion.12, f32[512,512]{1,0:T(8,128)S(1)} %bitcast.72), kind=kOutput, calls=%fused_computation.13 | convolution fusion | flops 1615069184 | bytes 2621440 | tf_op jit(solution)/shard_map/dot_general | solution.py:70
  123.4 2.1 %reduce.1 = bf16[512,512]{1,0:T(8,128)(2,1)S(1)} reduce(bf16[512,1,512]{2,0,1:T(8,128)(2,1)} %fusion.4, bf16[]{:T(256)} %broadcast.262), dimensions={1}, to_apply=%copy.40.reduce_sub_computation | reduce | bytes 1048578 | tf_op jit(solution)/shard_map/reshape | solution.py:72
  125.5 1.2 reshape.201
  126.6 4.0 %all-to-all-start.3 = ((bf16[32,2,4096]{2,1,0:T(2,128)(2,1)}), bf16[32,2,4096]{2,1,0:T(2,128)(2,1)}, u32[]{:S(2)}, u32[]{:S(2)}) async-start(bf16[32,2,4096]{2,1,0:T(2,128)(2,1)} %reshape.201), calls=%async_computation.3 | async-start | bytes 1048576 | tf_op jit(solution)/shard_map/all_to_all | solution.py:73
  130.6 9.4 %fusion.109 = f32[512,2048]{1,0:T(8,128)} fusion(bf16[512,2048]{1,0:T(8,128)(2,1)S(1)} %copy-done, bf16[2048,2048]{1,0:T(8,128)(2,1)} %param.7), kind=kOutput, calls=%fused_computation.130 | convolution fusion | flops 4294967296 | bytes 14680064 | tf_op jit(solution)/shard_map/dot_general | solution.py:76
  140.0 0.0 copy-start.4
  140.0 6.0 %all-to-all-done.3 = bf16[32,2,4096]{2,1,0:T(2,128)(2,1)} async-done(((bf16[32,2,4096]{2,1,0:T(2,128)(2,1)}), bf16[32,2,4096]{2,1,0:T(2,128)(2,1)}, u32[]{:S(2)}, u32[]{:S(2)}) %all-to-all-start.3) | async-done | bytes 524320 | tf_op jit(solution)/shard_map/all_to_all | solution.py:73
  146.0 3.6 %reshape.202 = bf16[512,1,512]{2,1,0:T(2,128)(2,1)S(1)} reshape(bf16[32,2,4096]{2,1,0:T(2,128)(2,1)} %all-to-all-done.3) | data formatting | bytes 1048576
  149.6 0.0 copy-start.3
  149.6 0.1 copy.48
  149.7 0.3 copy.41
  150.0 0.0 copy-done.4
  150.1 1.1 copy-done.3
  151.2 5.0 %multiply_convert_fusion = bf16[512,2048]{1,0:T(8,128)(2,1)} fusion(f32[512,2048]{1,0:T(8,128)} %fusion.109, bf16[512,512]{1,0:T(8,128)(2,1)S(1)} %bitcast.74, bf16[512,2048]{1,0:T(8,128)(2,1)S(1)} %copy-done.3, f32[2048]{0:T(1024)S(1)} %copy-done.4), kind=kOutput, calls=%fused_computation | convolution fusion | flops 1080033280 | bytes 8921088 | tf_op jit(solution)/shard_map/dot_general | solution.py:77
  (2 shorter events, 0.0 us)
Async XLA Ops:
  0.0 1.6 %copy-start = (bf16[512,2048]{1,0:T(8,128)(2,1)S(1)}, bf16[512,2048]{1,0:T(8,128)(2,1)}, u32[]{:S(2)}) copy-start(bf16[512,2048]{1,0:T(8,128)(2,1)} %param.5) | copy-start | bytes 6291460
  12.7 22.9 %all-to-all-start = ((bf16[32,2,4096]{2,1,0:T(2,128)(2,1)}), bf16[32,2,4096]{2,1,0:T(2,128)(2,1)S(1)}, u32[]{:S(2)}, u32[]{:S(2)}) async-start(bf16[32,2,4096]{2,1,0:T(2,128)(2,1)} %reshape.199), calls=%async_computation | async-start | bytes 1048576 | tf_op jit(solution)/shard_map/all_to_all | solution.py:33
  38.7 0.8 copy-start.2
  47.7 2.0 %copy-start.1 = (f32[32,16,4,128]{3,2,0,1:T(4,128)S(1)}, f32[32,16,4,128]{3,2,0,1:T(4,128)}, u32[]{:S(2)}) copy-start(f32[32,16,4,128]{3,2,0,1:T(4,128)} %reshape.187) | copy-start | bytes 3145732
  85.7 29.8 %all-to-all-start.2 = ((f32[32,16,512]{2,1,0:T(8,128)}), f32[32,16,512]{2,1,0:T(8,128)S(1)}, u32[]{:S(2)}, u32[]{:S(2)}) async-start(f32[32,16,512]{2,1,0:T(8,128)} %get-tuple-element.5), calls=%async_computation.2 | async-start | bytes 2097152 | tf_op jit(solution)/shard_map/all_to_all | solution.py:64
  126.6 19.3 %all-to-all-start.3 = ((bf16[32,2,4096]{2,1,0:T(2,128)(2,1)}), bf16[32,2,4096]{2,1,0:T(2,128)(2,1)}, u32[]{:S(2)}, u32[]{:S(2)}) async-start(bf16[32,2,4096]{2,1,0:T(2,128)(2,1)} %reshape.201), calls=%async_computation.3 | async-start | bytes 1048576 | tf_op jit(solution)/shard_map/all_to_all | solution.py:73
  140.0 10.0 %copy-start.4 = (f32[2048]{0:T(1024)S(1)}, f32[2048]{0:T(1024)}, u32[]{:S(2)}) copy-start(f32[2048]{0:T(1024)} %param.8) | copy-start | bytes 24580
  149.6 1.6 %copy-start.3 = (bf16[512,2048]{1,0:T(8,128)(2,1)S(1)}, bf16[512,2048]{1,0:T(8,128)(2,1)}, u32[]{:S(2)}) copy-start(bf16[512,2048]{1,0:T(8,128)(2,1)} %param.9) | copy-start | bytes 6291460
where the time goes:
time: 157 us; the launch traced here: 156 us
  matrix products  45.3 us (29%)
  waiting for transfers between devices  39.3 us (25%)
  blocking collectives  29.1 us (19%)
  local copies, waits for them, and re-layouts  18.9 us (12%)
  starting transfers between devices  15.4 us (10%)
  other arithmetic  8.03 us (5%)
    all_to_all x1, blocking collectives, shards(): lax.all_to_all(twist_re, ('row', 'col'), split_axis=0, concat_axis=1, til...  29.1 us
    all_to_all x1, waiting for transfers between devices, shards(): lax.all_to_all(twist_im, ('row', 'col'), split_axis=0, concat_axis=1, til...  18 us
    all_to_all x1, waiting for transfers between devices, shards(): lax.all_to_all(mixed_in.reshape(1, local_len, channels), ('row', 'col'),...  15.3 us
    unnamed x17, local copies, waits for them, and re-layouts  14.4 us
    dot_general x1, matrix products, shards(): jnp.dot(tokens, w_gate, preferred_element_type=jnp.float32) + gate_bias  9.37 us
    dot_general x1, matrix products, shards(): jnp.dot(cos_m, recv_re, precision=HIGH)  7.95 us
    dot_general x1, matrix products, shards(): jnp.dot(sin_m, recv_im, precision=HIGH)  7.84 us
    all_to_all x1, starting transfers between devices, shards(): lax.all_to_all(mixed_in.reshape(1, local_len, channels), ('row', 'col'),...  7.51 us
  transfers between devices with their start and end apart: 3, of which 3 were waited for; matrix products, arithmetic and copies ran while one was open for 11% of the time, Pallas kernels for 0%

commit v1 on v0

--- a/solution.py
+++ b/solution.py
@@ -70,8 +70,14 @@
     real_part = jnp.dot(cos_m, recv_re, precision=HIGH) + jnp.dot(sin_m, recv_im, precision=HIGH)
     real_part = real_part * (1.0 / math.sqrt(full_len * GROUP_DIM))
     freq_rows = real_part.astype(jnp.bfloat16).reshape(local_len, 1, channels)
-    spectrum = lax.all_to_all(
-        freq_rows, ("row", "col"), split_axis=0, concat_axis=1, tiled=True
+    spectrum = jnp.concatenate(
+        lax.all_to_all(
+            jnp.stack(jnp.split(freq_rows, lax.axis_size(("row", "col")), axis=0)),
+            ("row", "col"),
+            0,
+            0,
+        ),
+        axis=1,
     ).reshape(local_len, channels)
     gate = jax.nn.sigmoid(jnp.dot(tokens, w_gate, preferred_element_type=jnp.float32) + gate_bias)
     branch = jnp.dot(spectrum, w_branch, preferred_element_type=jnp.float32)

time: 157 us -> 168 us (1.070)
  local copies, waits for them, and re-layouts: 18.9 us -> 32.2 us
  other arithmetic: 8.03 us -> 5.97 us
    unnamed x17 -> x43, local copies, waits for them, and re-layouts: 14.4 us -> 27.1 us
    reshape x1 -> x0, other arithmetic: 2.06 us -> none  [shards(): freq_rows = real_part.astype(jnp.bfloat16).reshape(local_len, 1, channels)]
  transfers between devices with their start and end apart: 3 -> 3, of which waited for: 3 -> 3; matrix products, arithmetic and copies ran while one was open for 11% -> 10% of each run, Pallas kernels for 0% -> 0%
where the time goes in v1:
time: 168 us; the launch traced here: 167 us
  matrix products  45.3 us (27%)
  waiting for transfers between devices  39.3 us (23%)
  local copies, waits for them, and re-layouts  32.2 us (19%)
  blocking collectives  29.1 us (17%)
  starting transfers between devices  15.2 us (9%)
  other arithmetic  5.97 us (4%)
    all_to_all x1, blocking collectives, shards(): lax.all_to_all(twist_re, ('row', 'col'), split_axis=0, concat_axis=1, til...  29.1 us
    unnamed x43, local copies, waits for them, and re-layouts  27.1 us
    all_to_all x1, waiting for transfers between devices, shards(): lax.all_to_all(twist_im, ('row', 'col'), split_axis=0, concat_axis=1, til...  18 us
    all_to_all x1, waiting for transfers between devices, shards(): lax.all_to_all(mixed_in.reshape(1, local_len, channels), ('row', 'col'),...  15.3 us
    dot_general x1, matrix products, shards(): jnp.dot(tokens, w_gate, preferred_element_type=jnp.float32) + gate_bias  9.39 us
    dot_general x1, matrix products, shards(): jnp.dot(cos_m, recv_re, precision=HIGH)  7.94 us
    all_to_all x1, starting transfers between devices, shards(): lax.all_to_all(mixed_in.reshape(1, local_len, channels), ('row', 'col'),...  7.51 us
    dot_general x1, matrix products, shards(): jnp.dot(sin_m, recv_im, precision=HIGH)  7.14 us
  transfers between devices with their start and end apart: 3, of which 3 were waited for; matrix products, arithmetic and copies ran while one was open for 10% of the time, Pallas kernels for 0%

profile of v1, /device:TPU:0, one launch (start us, length us, event | category | flops | bytes accessed | tf_op | source)
XLA Modules:
  0.0 167.3 jit_solution(13768814944732269448)
XLA Ops:
  0.0 1.6 copy-done
  1.6 2.8 %fusion.4 = bf16[1,512,512]{2,1,0:T(8,128)(2,1)S(1)} fusion(bf16[512,2048]{1,0:T(8,128)(2,1)S(1)} %copy-done, bf16[2048,512]{1,0:T(8,128)(2,1)} %param.6), kind=kOutput, calls=%fused_computation.13 | convolution fusion | flops 1074003968 | bytes 4718592 | tf_op jit(solution)/shard_map/dot_general | solution.py:30
  4.4 0.8 copy.66
  5.8 4.6 %reduce = bf16[512,512]{1,0:T(8,128)(2,1)} reduce(bf16[512,1,512]{2,1,0:T(2,128)(2,1)S(1)} %bitcast.194, bf16[]{:T(256)} %broadcast.262), dimensions={1}, to_apply=%bitcast.190.reduce_sub_computation | reduce | bytes 1048578
  10.4 2.2 %reshape.259 = bf16[32,2,4096]{2,1,0:T(2,128)(2,1)} reshape(bf16[512,512]{1,0:T(8,128)(2,1)} %reduce) | data formatting | bytes 1048576
  12.6 7.5 %all-to-all-start = ((bf16[32,2,4096]{2,1,0:T(2,128)(2,1)}), bf16[32,2,4096]{2,1,0:T(2,128)(2,1)S(1)}, u32[]{:S(2)}, u32[]{:S(2)}) async-start(bf16[32,2,4096]{2,1,0:T(2,128)(2,1)} %reshape.259), calls=%async_computation | async-start | bytes 1048576 | tf_op jit(solution)/shard_map/all_to_all | solution.py:33
  20.2 15.3 %all-to-all-done = bf16[32,2,4096]{2,1,0:T(2,128)(2,1)S(1)} async-done(((bf16[32,2,4096]{2,1,0:T(2,128)(2,1)}), bf16[32,2,4096]{2,1,0:T(2,128)(2,1)S(1)}, u32[]{:S(2)}, u32[]{:S(2)}) %all-to-all-start) | async-done | bytes 524320 | tf_op jit(solution)/shard_map/all_to_all | solution.py:33
  35.6 1.8 %reshape.260 = bf16[512,1,512]{2,1,0:T(2,128)(2,1)} reshape(bf16[32,2,4096]{2,1,0:T(2,128)(2,1)S(1)} %all-to-all-done) | data formatting | bytes 1048576
  37.3 1.3 copy.46
  38.7 0.8 copy-done.2
  39.5 0.9 reshape.258
  40.4 1.8 %fusion.22 = f32[32,16,4,128]{3,0,2,1:T(8,128)S(1)} fusion(bf16[16,4,128,32]{2,1,0,3:T(4,128)(2,1)} %reshape.258), kind=kOutput, calls=%fused_computation.35 | convolution fusion | flops 100677632 | bytes 1572864 | tf_op jit(solution)/shard_map/kn,nmc->kmc/dot_general | solution.py:43
  42.2 2.9 %convolution_negate_fusion = f32[32,16,512]{2,0,1:T(8,128)} fusion(bf16[32,16,512]{2,1,0:T(8,128)(2,1)} %bitcast.192), kind=kOutput, calls=%fused_computation.4 | convolution fusion | flops 100939776 | bytes 1572864 | tf_op jit(solution)/shard_map/kn,nmc->kmc/dot_general | solution.py:44
  45.1 2.5 %reshape.248 = f32[32,16,4,128]{3,2,0,1:T(4,128)} reshape(f32[32,16,512]{2,0,1:T(8,128)} %convolution_negate_fusion) | data formatting | bytes 2097152 | tf_op jit(solution)/shard_map/reshape | solution.py:48
  47.6 2.0 %fusion.20 = f32[32,16,4,128]{3,1,2,0:T(8,128)S(1)} fusion(f32[32,16,4,128]{3,0,2,1:T(8,128)S(1)} %fusion.22, s32[128]{0:T(128)S(1)} %get-tuple-element.9, s32[128]{0:T(128)S(1)} %get-tuple-element.10), kind=kOutput, calls=%fused_computation.33 | convolution fusion | flops 402915328 | bytes 2098176 | tf_op jit(solution)/shard_map/kmgc,cd->kmgd/dot_general | solution.py:49
  49.6 1.8 %fusion.16 = f32[32,16,4,128]{3,1,2,0:T(8,128)S(1)} fusion(f32[32,16,4,128]{3,2,0,1:T(4,128)S(1)} %copy-done.1, s32[128]{0:T(128)S(1)} %get-tuple-element.9, s32[128]{0:T(128)S(1)} %get-tuple-element.10), kind=kOutput, calls=%fused_computation.29 | convolution fusion | flops 402915328 | bytes 2098176 | tf_op jit(solution)/shard_map/kmgc,cd->kmgd/dot_general | solution.py:52
  51.4 1.8 %fusion.2 = f32[32,4,2,8,128]{4,3,2,1,0:T(8,128)S(1)} fusion(f32[32,16,4,128]{3,1,2,0:T(8,128)S(1)} %fusion.20, f32[32,16,4,128]{3,2,0,1:T(4,128)S(1)} %copy-done.1, s32[128]{0:T(128)S(1)} %get-tuple-element.9, s32[128]{0:T(128)S(1)} %get-tuple-element.10), kind=kOutput, calls=%fused_computation.10 | convolution fusion | flops 403177472 | bytes 3146752 | tf_op jit(solution)/shard_map/kmgc,cd->kmgd/dot_general | solution.py:49
  53.3 2.0 %fusion.1 = f32[32,4,2,8,128]{4,3,2,1,0:T(8,128)S(1)} fusion(f32[32,16,4,128]{3,1,2,0:T(8,128)S(1)} %fusion.16, f32[32,16,4,128]{3,0,2,1:T(8,128)S(1)} %fusion.22, s32[128]{0:T(128)S(1)} %get-tuple-element.9, s32[128]{0:T(128)S(1)} %get-tuple-element.10), kind=kOutput, calls=%fused_computation.8 | convolution fusion | flops 403177472 | bytes 3146752 | tf_op jit(solution)/shard_map/kmgc,cd->kmgd/dot_general | solution.py:52
  55.3 1.3 fusion.9
  56.6 29.1 %all_to_all.35 = f32[32,16,512]{2,1,0:T(8,128)} all-to-all(f32[32,16,512]{2,1,0:T(8,128)S(1)} %get-tuple-element.6), channel_id=1, replica_groups=mesh['row'=8,'col'=4] {'row','col'}, dimensions={0} | all-to-all | bytes 2097152 | tf_op jit(solution)/shard_map/all_to_all | solution.py:63
  85.7 3.8 %all-to-all-start.2 = ((f32[32,16,512]{2,1,0:T(8,128)}), f32[32,16,512]{2,1,0:T(8,128)S(1)}, u32[]{:S(2)}, u32[]{:S(2)}) async-start(f32[32,16,512]{2,1,0:T(8,128)} %get-tuple-element.5), calls=%async_computation.2 | async-start | bytes 2097152 | tf_op jit(solution)/shard_map/all_to_all | solution.py:64
  89.5 7.9 %fusion.11 = f32[512,512]{1,0:T(8,128)} fusion(f32[512,512]{1,0:T(8,128)} %bitcast.197), kind=kOutput, calls=%fused_computation.24 | convolution fusion | flops 1614282752 | bytes 2097152 | tf_op jit(solution)/shard_map/dot_general | solution.py:70
  97.4 18.0 %all-to-all-done.2 = f32[32,16,512]{2,1,0:T(8,128)S(1)} async-done(((f32[32,16,512]{2,1,0:T(8,128)}), f32[32,16,512]{2,1,0:T(8,128)S(1)}, u32[]{:S(2)}, u32[]{:S(2)}) %all-to-all-start.2) | async-done | bytes 1048608 | tf_op jit(solution)/shard_map/all_to_all | solution.py:64
  115.5 7.1 %fusion.3 = bf16[512,512]{1,0:T(8,128)(2,1)S(1)} fusion(f32[512,512]{1,0:T(8,128)} %fusion.11, f32[512,512]{1,0:T(8,128)S(1)} %bitcast.196), kind=kOutput, calls=%fused_computation.12 | convolution fusion | flops 1615069184 | bytes 2621440 | tf_op jit(solution)/shard_map/dot_general | solution.py:70
  122.6 0.6 constant_dynamic-update-slice_fusion.31
  123.3 0.6 constant_dynamic-update-slice_fusion.30
  123.9 0.6 constant_dynamic-update-slice_fusion.29
  124.5 0.6 constant_dynamic-update-slice_fusion.28
  126.3 0.6 constant_dynamic-update-slice_fusion.25
  126.9 0.6 constant_dynamic-update-slice_fusion.24
  127.5 0.6 constant_dynamic-update-slice_fusion.23
  128.1 0.6 constant_dynamic-update-slice_fusion.22
  128.7 0.6 constant_dynamic-update-slice_fusion.21
  129.3 0.6 constant_dynamic-update-slice_fusion.20
  129.9 0.6 constant_dynamic-update-slice_fusion.19
  130.5 0.6 constant_dynamic-update-slice_fusion.18
  132.4 0.6 constant_dynamic-update-slice_fusion.15
  133.0 0.6 constant_dynamic-update-slice_fusion.14
  133.6 0.6 constant_dynamic-update-slice_fusion.13
  134.2 0.6 constant_dynamic-update-slice_fusion.12
  134.8 0.6 constant_dynamic-update-slice_fusion.11
  135.4 0.6 constant_dynamic-update-slice_fusion.10
  136.0 0.6 constant_dynamic-update-slice_fusion.9
  137.8 0.6 constant_dynamic-update-slice_fusion.6
  142.1 3.9 %all-to-all-start.3 = ((bf16[32,16,1,512]{3,1,2,0:T(8,128)(2,1)}), bf16[32,16,1,512]{3,1,2,0:T(8,128)(2,1)S(1)}, u32[]{:S(2)}, u32[]{:S(2)}) async-start(bf16[32,16,1,512]{3,1,2,0:T(8,128)(2,1)} %constant_dynamic-update-slice_fusion), calls=%async_computation.3 | async-start | bytes 1048576 | tf_op jit(solution)/shard_map/all_to_all | solution.py:74
  146.0 9.4 %fusion.108 = f32[512,2048]{1,0:T(8,128)} fusion(bf16[512,2048]{1,0:T(8,128)(2,1)S(1)} %copy-done, bf16[2048,2048]{1,0:T(8,128)(2,1)} %param.7), kind=kOutput, calls=%fused_computation.193 | convolution fusion | flops 4294967296 | bytes 14680064 | tf_op jit(solution)/shard_map/dot_general | solution.py:82
  155.4 5.9 %all-to-all-done.3 = bf16[32,16,1,512]{3,1,2,0:T(8,128)(2,1)S(1)} async-done(((bf16[32,16,1,512]{3,1,2,0:T(8,128)(2,1)}), bf16[32,16,1,512]{3,1,2,0:T(8,128)(2,1)S(1)}, u32[]{:S(2)}, u32[]{:S(2)}) %all-to-all-start.3) | async-done | bytes 524320 | tf_op jit(solution)/shard_map/all_to_all | solution.py:74
  161.6 5.6 %multiply_convert_fusion = bf16[512,2048]{1,0:T(8,128)(2,1)} fusion(f32[512,2048]{1,0:T(8,128)} %fusion.108, bf16[512,512]{1,0:T(8,128)(2,1)S(1)} %bitcast.198, bf16[512,2048]{1,0:T(8,128)(2,1)} %param.9, f32[2048]{0:T(1024)S(1)} %copy-done.3), kind=kOutput, calls=%fused_computation | convolution fusion | flops 1080033280 | bytes 8921088 | tf_op jit(solution)/shard_map/dot_general | solution.py:83
  (23 shorter events, 8.2 us)
Async XLA Ops:
  0.0 1.6 copy-start
  12.6 22.9 %all-to-all-start = ((bf16[32,2,4096]{2,1,0:T(2,128)(2,1)}), bf16[32,2,4096]{2,1,0:T(2,128)(2,1)S(1)}, u32[]{:S(2)}, u32[]{:S(2)}) async-start(bf16[32,2,4096]{2,1,0:T(2,128)(2,1)} %reshape.259), calls=%async_computation | async-start | bytes 1048576 | tf_op jit(solution)/shard_map/all_to_all | solution.py:33
  38.7 0.8 copy-start.2
  47.6 2.0 %copy-start.1 = (f32[32,16,4,128]{3,2,0,1:T(4,128)S(1)}, f32[32,16,4,128]{3,2,0,1:T(4,128)}, u32[]{:S(2)}) copy-start(f32[32,16,4,128]{3,2,0,1:T(4,128)} %reshape.248) | copy-start | bytes 3145732
  85.7 29.8 %all-to-all-start.2 = ((f32[32,16,512]{2,1,0:T(8,128)}), f32[32,16,512]{2,1,0:T(8,128)S(1)}, u32[]{:S(2)}, u32[]{:S(2)}) async-start(f32[32,16,512]{2,1,0:T(8,128)} %get-tuple-element.5), calls=%async_computation.2 | async-start | bytes 2097152 | tf_op jit(solution)/shard_map/all_to_all | solution.py:64
  142.1 19.2 %all-to-all-start.3 = ((bf16[32,16,1,512]{3,1,2,0:T(8,128)(2,1)}), bf16[32,16,1,512]{3,1,2,0:T(8,128)(2,1)S(1)}, u32[]{:S(2)}, u32[]{:S(2)}) async-start(bf16[32,16,1,512]{3,1,2,0:T(8,128)(2,1)} %constant_dynamic-update-slice_fusion), calls=%async_computation.3 | async-start | bytes 1048576 | tf_op jit(solution)/shard_map/all_to_all | solution.py:74
  146.0 15.7 %copy-start.3 = (f32[2048]{0:T(1024)S(1)}, f32[2048]{0:T(1024)}, u32[]{:S(2)}) copy-start(f32[2048]{0:T(1024)} %param.8) | copy-start | bytes 24580
